TPU v7x, 256 devices: a whole 4x4x8 slice. The times are simulated.
256 devices in a mesh: rep: 2 (over z_hi), fs: 16 (over z_lo, x), tp: 8 (over y, core).
Axes of the slice: x: 4, y: 4, z: 8 (z_hi: 2, z_lo: 4; z = z_hi * 4 + z_lo), core: 2. Of those that a mesh axis runs over, the one named last changes fastest.
Arguments:
- tokens: bfloat16 [32, 1024, 2048], P(('rep', 'fs')), may hold values from -6 to 6
- mix_gain: bfloat16 [2048], replicated, may hold values from 0.099609375 to 1.8984375
- value_weight: bfloat16 [2048, 1024], P('fs', 'tp'), may hold values from -0.125 to 0.125
- gate_weight: bfloat16 [2048, 1024], P('fs', 'tp'), may hold values from -0.125 to 0.125
- mix_taps: bfloat16 [31, 1024], P(None, 'tp'), may hold values from -1 to 1
- head_gain: bfloat16 [1024], P('tp'), may hold values from 0.099609375 to 1.8984375
- out_weight: bfloat16 [1024, 2048], P('fs', 'tp'), may hold values from -0.1875 to 0.1875
- ffn_gain: bfloat16 [2048], replicated, may hold values from 0.099609375 to 1.8984375
- ffgate_weight: bfloat16 [2048, 6144], P('fs', 'tp'), may hold values from -0.125 to 0.125
- up_weight: bfloat16 [2048, 6144], P('fs', 'tp'), may hold values from -0.125 to 0.125
- ff_taps: bfloat16 [3, 6144], P(None, 'tp'), may hold values from -3.5 to 3.5
- down_weight: bfloat16 [2048, 6144], P('fs', 'tp'), may hold values from -0.078125 to 0.078125
Outputs:
- layer_out: bfloat16 [32, 1024, 2048], P(('rep', 'fs'), 'tp')
All inputs are finite; a program needn't handle non-finite values.
Results may differ from a plain program's by a relative error of at most 0.01.
Values may be sent and summed in bfloat16 or wider, within the bound.
A program may use at most 64 MiB of HBM per device.

v0:
```python
import jax
import jax.numpy as jnp
from jax import lax
from jax.sharding import PartitionSpec as P

HEAD = 128
norm_floor = 0.01


def in_one_piece(arrays, axis, dim, along):
    both = jnp.concatenate(arrays, axis=along)
    result, at, finished = (lax.all_gather(both, axis, axis=dim, tiled=True), 0, [])
    for a in arrays:
        finished.append(lax.slice_in_dim(result, at, at + a.shape[along], axis=along))
        at += a.shape[along]
    return tuple(finished)


def laid_out(parts, dim):
    lengths = list(parts.shape[1:])
    lengths[dim] *= parts.shape[0]
    return jnp.moveaxis(parts, 0, dim).reshape(lengths)


def sent_to_all(value, axis):
    count = lax.axis_size(axis)
    return lax.all_to_all(
        jnp.broadcast_to(value[None], (count, *value.shape)), axis, 0, 0, tiled=True
    )


def collect(value, axis, dim):
    return laid_out(sent_to_all(value, axis), dim)


def row_norm(floats_in, scales):
    floats = floats_in.astype(jnp.float32)
    scaled = floats * lax.rsqrt(jnp.mean(floats * floats, axis=-1, keepdims=True) + norm_floor)
    return (scaled * scales.astype(jnp.float32)).astype(jnp.bfloat16)


def causal_conv(signal, kernel_taps):
    reach = kernel_taps.shape[0]
    length = signal.shape[0]
    padded = jnp.pad(signal, ((reach - 1, 0), (0, 0)))
    summed = padded[0:length] * kernel_taps[0]
    for offset in range(1, reach):
        summed = summed + padded[offset : offset + length] * kernel_taps[offset]
    return summed


def head_norm(signal, scales):
    length = signal.shape[0]
    grouped = signal.reshape(length, signal.shape[1] // HEAD, HEAD)
    centre = grouped - jnp.mean(grouped, axis=-1, keepdims=True)
    spread = jnp.mean(centre * centre, axis=-1, keepdims=True)
    normal = (centre * lax.rsqrt(spread + norm_floor)).reshape(signal.shape)
    return normal * scales.astype(jnp.float32)


def on_device(
    tokens,
    mix_gain,
    value_weight,
    gate_weight,
    mix_taps,
    head_gain,
    out_weight,
    ffn_gain,
    ffgate_weight,
    up_weight,
    ff_taps,
    down_weight,
):
    sequence = tokens[0]
    value_full, gate_full, out_full = (
        *in_one_piece((value_weight, gate_weight), "fs", 0, 1),
        lax.all_gather(out_weight, "fs", axis=0, tiled=True),
    )
    normed = row_norm(sequence, mix_gain)
    values = jnp.dot(normed, value_full, preferred_element_type=jnp.float32)
    gating = jnp.dot(normed, gate_full, preferred_element_type=jnp.float32)
    glu_out = values * jax.nn.sigmoid(gating)
    mixed_pos = causal_conv(glu_out, mix_taps.astype(jnp.float32))
    head_out = jax.nn.silu(head_norm(mixed_pos, head_gain)).astype(jnp.bfloat16)
    out_cols = out_full.shape[1]
    mixer_sum = jnp.dot(collect(head_out, "tp", 1), out_full, preferred_element_type=jnp.float32)
    own_cols = lax.dynamic_slice_in_dim(sequence, lax.axis_index("tp") * out_cols, out_cols, 1)
    hidden_cols = (own_cols.astype(jnp.float32) + mixer_sum).astype(jnp.bfloat16)
    full_rows = collect(hidden_cols, "tp", 1)
    normed_ffn = row_norm(full_rows, ffn_gain)
    ffgate_full, up_full, down_full = in_one_piece(
        (ffgate_weight, up_weight, down_weight), "fs", 0, 1
    )
    ffgate = jnp.dot(normed_ffn, ffgate_full, preferred_element_type=jnp.float32)
    ff_up = jnp.dot(normed_ffn, up_full, preferred_element_type=jnp.float32)
    product = (jax.nn.silu(causal_conv(ffgate, ff_taps.astype(jnp.float32))) * ff_up).astype(
        jnp.bfloat16
    )
    own_count = sequence.shape[0] // lax.axis_size("tp")
    summed_rows = lax.psum_scatter(
        lax.dot_general(
            product, down_full, (((1,), (1,)), ((), ())), preferred_element_type=jnp.float32
        ).astype(jnp.bfloat16),
        "tp",
        scatter_dimension=0,
        tiled=True,
    ).astype(jnp.float32)
    own_rows = lax.dynamic_slice_in_dim(full_rows, lax.axis_index("tp") * own_count, own_count, 0)
    return (own_rows.astype(jnp.float32) + summed_rows).astype(jnp.bfloat16)[None]


def solution(mesh):
    placed = (
        P(("rep", "fs"), None, None),
        P(),
        P("fs", "tp"),
        P("fs", "tp"),
        P(None, "tp"),
        P("tp"),
        P("fs", "tp"),
        P(),
        P("fs", "tp"),
        P("fs", "tp"),
        P(None, "tp"),
        P("fs", "tp"),
    )
    return jax.shard_map(
        on_device,
        mesh=mesh,
        in_specs=placed,
        out_specs=P(("rep", "fs"), "tp", None),
        check_vma=False,
    )
```

profile of v0, /device:TPU:2, one launch (start us, length us, event | category | flops | bytes accessed | tf_op | source)
XLA Modules:
  0.0 288.3 jit_solution(5631899836314753559)
XLA Ops:
  6.5 0.0 all-gather.3.cloned.1.call-start
  6.5 1.4 pad_maximum_fusion.1
  7.9 0.0 all-gather.3.cloned.1.call-update
  8.0 0.0 all-gather.5.cloned.1.call-start
  8.0 2.0 pad_maximum_fusion
  10.0 0.0 all-gather.5.cloned.1.call-update
  10.0 0.7 convert_element_type.73
  10.7 0.7 convert_element_type.70
  11.4 0.7 convert_element_type.72
  12.1 3.1 %fusion = f32[1024]{0:T(1024)S(1)} fusion(bf16[1,1024,2048]{2,1,0:T(8,128)(2,1)} %param.12), kind=kLoop, calls=%fused_computation.2 | loop fusion | flops 6290432 | bytes 4198400 | tf_op jit(solution)/shard_map/reduce_sum | solution.py:38
  15.2 77.5 %all-gather.3.cloned.1.call-done = bf16[2048,256]{1,0:T(8,128)(2,1)} async-done(((bf16[128,256]{1,0:T(8,128)(2,1)}), bf16[2048,256]{1,0:T(8,128)(2,1)}) %all-gather.3.cloned.1.call-update) | async-done | bytes 1048592 | tf_op jit(solution)/shard_map/all_gather | solution.py:12
  92.7 0.0 copy-start
  92.7 0.0 copy-start.4
  92.7 3.8 %fusion.19 = f32[1024,128]{1,0:T(8,128)S(1)} fusion(bf16[1,1024,2048]{2,1,0:T(8,128)(2,1)} %param.12, f32[2048]{0:T(1024)S(1)} %convert_element_type.70, f32[1024]{0:T(1024)S(1)} %add_rsqrt_fusion.2, bf16[2048,256]{1,0:T(8,128)(2,1)} %all-gather.3.cloned.1.call-done), kind=kOutput, calls=%fused_computation.24 | convolution fusion | flops 545652736 | bytes 5255168 | tf_op jit(solution)/shard_map/dot_general | solution.py:82
  96.5 0.0 copy-done
  96.5 0.1 copy-done.4
  96.6 1.3 convolution_multiply_fusion
  98.0 2.3 fusion.48
  100.3 0.0 copy-start.1
  100.3 0.4 multiply_reduce_fusion.1
  100.7 0.4 multiply_convert_fusion.5
  101.0 0.1 copy.14
  101.2 1.6 broadcast_in_dim.6
  102.8 4.3 %all-to-all-start = ((bf16[8,1024,128]{1,2,0:T(8,128)(2,1)}), bf16[8,1024,128]{1,2,0:T(8,128)(2,1)S(1)}, u32[]{:S(2)}, u32[]{:S(2)}) async-start(bf16[8,1024,128]{1,2,0:T(8,128)(2,1)} %broadcast_in_dim.6), calls=%async_computation | async-start | bytes 4194304 | tf_op jit(solution)/shard_map/all_to_all | solution.py:27
  107.1 0.0 copy-done.1
  107.1 46.9 %all_gather.10 = bf16[1024,256]{1,0:T(8,128)(2,1)S(1)} all-gather(bf16[64,256]{1,0:T(8,128)(2,1)S(1)} %copy-done.1), channel_id=1, replica_groups=mesh['rep'=2,'fs'=16,'tp'=8] {'fs'}, dimensions={0}, use_global_device_ids=true | all-gather | bytes 557056 | tf_op jit(solution)/shard_map/all_gather | solution.py:78
  153.9 0.0 all-to-all-done
  153.9 1.8 fusion.16
  155.8 2.3 broadcast_in_dim.7
  158.1 0.0 copy-start.3
  158.1 0.0 copy-start.2
  158.1 5.0 %all-to-all-start.1 = ((bf16[8,1024,256]{2,1,0:T(8,128)(2,1)}), bf16[8,1024,256]{2,1,0:T(8,128)(2,1)}, u32[]{:S(2)}, u32[]{:S(2)}) async-start(bf16[8,1024,256]{2,1,0:T(8,128)(2,1)} %broadcast_in_dim.7), calls=%async_computation.1 | async-start | bytes 8388608 | tf_op jit(solution)/shard_map/all_to_all | solution.py:27
  163.1 0.2 reduce-scatter.2.cloned.1.call-start
  163.3 0.0 copy-done.3
  163.3 0.0 copy-done.2
  163.4 49.4 %all-to-all-done.1 = bf16[8,1024,256]{2,1,0:T(8,128)(2,1)} async-done(((bf16[8,1024,256]{2,1,0:T(8,128)(2,1)}), bf16[8,1024,256]{2,1,0:T(8,128)(2,1)}, u32[]{:S(2)}, u32[]{:S(2)}) %all-to-all-start.1) | async-done | bytes 4194336 | tf_op jit(solution)/shard_map/all_to_all | solution.py:27
  212.8 4.8 %copy.16 = bf16[8,128,8,256]{3,2,0,1:T(8,128)(2,1)} copy(bf16[8,128,8,256]{3,2,1,0:T(8,128)(2,1)} %bitcast.40) | data formatting | bytes 8388608 | tf_op jit(solution)/shard_map/reshape | solution.py:22
  217.6 3.1 %multiply_reduce_fusion = f32[1024]{0:T(1024)S(1)} fusion(bf16[8,1024,256]{2,1,0:T(8,128)(2,1)} %all-to-all-done.1), kind=kLoop, calls=%fused_computation.6 | loop fusion | flops 6290432 | bytes 4198400 | tf_op jit(solution)/shard_map/reduce_sum | solution.py:38
  220.7 0.0 all-gather.5.cloned.1.call-done
  220.8 6.4 %fusion.6 = f32[1024,768]{1,0:T(8,128)S(1)} fusion(bf16[2048,2304]{1,0:T(8,128)(2,1)} %all-gather.5.cloned.1.call-done, bf16[1024,2048]{1,0:T(8,128)(2,1)} %bitcast.82, f32[2048]{0:T(1024)S(1)} %convert_element_type.79, f32[1024]{0:T(1024)S(1)} %add_rsqrt_fusion), kind=kOutput, calls=%fused_computation.11 | convolution fusion | flops 3229614080 | bytes 10498048 | tf_op jit(solution)/shard_map/dot_general | solution.py:95
  227.2 13.3 %convolution_convert_fusion = bf16[1024,2048]{1,0:T(8,128)(2,1)} fusion(bf16[2048,2304]{1,0:T(8,128)(2,1)} %all-gather.5.cloned.1.call-done, f32[1024,768]{1,0:T(8,128)S(1)} %fusion.6, f32[768]{0:T(1024)S(1)} %get-tuple-element.6, f32[768]{0:T(1024)S(1)} %get-tuple-element.7, f32[768]{0:T(1024)S(1)} %get-tuple-element.5, bf16[1024,2048]{1,0:T(8,128)(2,1)} %bitcast.83, ...), kind=kOutput, calls=%fused_computation.7 | convolution fusion | flops 6461587456 | bytes 17847296 | tf_op jit(solution)/shard_map/dot_general | solution.py:102
  240.5 0.0 reduce-scatter.2.cloned.1.call-update
  240.6 39.1 %reduce-scatter.2.cloned.1.call-done = bf16[128,2048]{1,0:T(8,128)(2,1)} async-done(((bf16[1024,2048]{1,0:T(8,128)(2,1)}), bf16[128,2048]{1,0:T(8,128)(2,1)}) %reduce-scatter.2.cloned.1.call-update) | async-done | bytes 524304 | tf_op jit(solution)/shard_map/reduce_scatter | solution.py:101
  279.6 2.1 fusion.22
  (9 shorter events, 0.1 us)
Async XLA Ops:
  6.5 86.2 %all-gather.3.cloned.1.call-start = ((), (), s32[]{:S(2)}) async-start(), calls=%async_computation.3 | async-start | bytes 1114112 | tf_op jit(solution)/shard_map/all_gather | solution.py:12
  8.0 212.8 %all-gather.5.cloned.1.call-start = ((), (), s32[]{:S(2)}) async-start(), calls=%async_computation.4 | async-start | bytes 10027008 | tf_op jit(solution)/shard_map/all_gather | solution.py:12
  92.7 3.8 %copy-start = (bf16[1,1024,2048]{2,1,0:T(8,128)(2,1)S(1)}, bf16[1,1024,2048]{2,1,0:T(8,128)(2,1)}, u32[]{:S(2)}) copy-start(bf16[1,1024,2048]{2,1,0:T(8,128)(2,1)} %param.12) | copy-start | bytes 12582916
  92.7 3.9 %copy-start.4 = (bf16[2048,256]{1,0:T(8,128)(2,1)S(1)}, bf16[2048,256]{1,0:T(8,128)(2,1)}, u32[]{:S(2)}) copy-start(bf16[2048,256]{1,0:T(8,128)(2,1)} %all-gather.3.cloned.1.call-done) | copy-start | bytes 3145732
  100.3 6.8 %copy-start.1 = (bf16[64,256]{1,0:T(8,128)(2,1)S(1)}, bf16[64,256]{1,0:T(8,128)(2,1)}, u32[]{:S(2)}) copy-start(bf16[64,256]{1,0:T(8,128)(2,1)} %param.18) | copy-start | bytes 98308
  102.8 51.2 %all-to-all-start = ((bf16[8,1024,128]{1,2,0:T(8,128)(2,1)}), bf16[8,1024,128]{1,2,0:T(8,128)(2,1)S(1)}, u32[]{:S(2)}, u32[]{:S(2)}) async-start(bf16[8,1024,128]{1,2,0:T(8,128)(2,1)} %broadcast_in_dim.6), calls=%async_computation | async-start | bytes 4194304 | tf_op jit(solution)/shard_map/all_to_all | solution.py:27
  158.1 5.2 %copy-start.3 = (bf16[2048]{0:T(1024)(128)(2,1)S(1)}, bf16[2048]{0:T(1024)(128)(2,1)}, u32[]{:S(2)}) copy-start(bf16[2048]{0:T(1024)(128)(2,1)} %param.19) | copy-start | bytes 12292
  158.1 5.2 %copy-start.2 = (bf16[3,768]{1,0:T(4,128)(2,1)S(1)}, bf16[3,768]{1,0:T(4,128)(2,1)}, u32[]{:S(2)}) copy-start(bf16[3,768]{1,0:T(4,128)(2,1)} %param.22) | copy-start | bytes 13828
  158.1 54.7 %all-to-all-start.1 = ((bf16[8,1024,256]{2,1,0:T(8,128)(2,1)}), bf16[8,1024,256]{2,1,0:T(8,128)(2,1)}, u32[]{:S(2)}, u32[]{:S(2)}) async-start(bf16[8,1024,256]{2,1,0:T(8,128)(2,1)} %broadcast_in_dim.7), calls=%async_computation.1 | async-start | bytes 8388608 | tf_op jit(solution)/shard_map/all_to_all | solution.py:27
  163.1 116.6 %reduce-scatter.2.cloned.1.call-start = ((), (), s32[]{:S(2)}) async-start(), calls=%async_computation.5 | async-start | bytes 4718592 | tf_op jit(solution)/shard_map/reduce_scatter | solution.py:101
Sparse Core Ops, SparseCore 0:
  9.1 83.5 all-gather.2
  94.5 114.2 all-gather.4
  240.7 38.8 reduce-scatter.1
where the time goes:
time: 289 us; the launch traced here: 288 us
  waiting for transfers between devices  166 us (57%)
  blocking collectives  46.9 us (16%)
  matrix products  26.7 us (9%)
  other arithmetic  16.8 us (6%)
  between operations  13.3 us (5%)
  starting transfers between devices  9.5 us (3%)
  local copies, waits for them, and re-layouts  9.09 us (3%)
    all_gather x2, waiting for transfers between devices, in_one_piece(): lax.all_gather(both, axis, axis=dim, tiled=True)  77.6 us
    all_to_all x2, waiting for transfers between devices, sent_to_all(): lax.all_to_all(jnp.broadcast_to(value[None], (count, *value.shape)), axis...  49.4 us
    all_gather x1, blocking collectives, on_device(): lax.all_gather(out_weight, 'fs', axis=0, tiled=True)  46.9 us
    reduce_scatter x1, waiting for transfers between devices, on_device(): lax.psum_scatter(lax.dot_general(product, down_full, (((1,), (1,)), ((),...  39.1 us
    dot_general x1, matrix products, on_device(): lax.dot_general(product, down_full, (((1,), (1,)), ((), ())), preferred_e...  13.3 us
    all_to_all x2, starting transfers between devices, sent_to_all(): lax.all_to_all(jnp.broadcast_to(value[None], (count, *value.shape)), axis...  9.24 us
    dot_general x1, matrix products, on_device(): jnp.dot(normed_ffn, ffgate_full, preferred_element_type=jnp.float32)  6.42 us
    reduce_sum x2, other arithmetic, row_norm(): jnp.mean(floats * floats, axis=-1, keepdims=True) + norm_floor  6.14 us
  transfers between devices with their start and end apart: 5, of which 3 were waited for; matrix products, arithmetic and copies ran while one was open for 10% of the time, Pallas kernels for 0%

commit v1 on v0

--- a/solution.py
+++ b/solution.py
@@ -75,7 +75,9 @@
     sequence = tokens[0]
     value_full, gate_full, out_full = (
         *in_one_piece((value_weight, gate_weight), "fs", 0, 1),
-        lax.all_gather(out_weight, "fs", axis=0, tiled=True),
+        jnp.concatenate(
+            lax.all_to_all(jnp.stack([out_weight] * lax.axis_size("fs")), "fs", 0, 0), axis=0
+        ),
     )
     normed = row_norm(sequence, mix_gain)
     values = jnp.dot(normed, value_full, preferred_element_type=jnp.float32)

time: 289 us -> 273 us (0.945)
  blocking collectives: 46.9 us -> 0 us
  waiting for transfers between devices: 166 us -> 187 us
  starting transfers between devices: 9.5 us -> 18.1 us
    all_gather x1 -> x0, blocking collectives: 46.9 us -> none  [on_device(): lax.all_gather(out_weight, 'fs', axis=0, tiled=True)]
    all_to_all x2, waiting for transfers between devices: 49.4 us -> 76.5 us  [sent_to_all(): lax.all_to_all(jnp.broadcast_to(value[None], (count, *value.shape)), axis...]
    all_to_all x0 -> x1, starting transfers between devices: none -> 8.91 us  [on_device(): lax.all_to_all(jnp.stack([out_weight] * lax.axis_size('fs')), 'fs', 0, 0)]
    all_gather x2, waiting for transfers between devices: 77.6 us -> 69.8 us  [in_one_piece(): lax.all_gather(both, axis, axis=dim, tiled=True)]
  transfers between devices with their start and end apart: 5 -> 6, of which waited for: 3 -> 5; matrix products, arithmetic and copies ran while one was open for 10% -> 11% of each run, Pallas kernels for 0% -> 0%
where the time goes in v1:
time: 273 us; the launch traced here: 272 us
  waiting for transfers between devices  187 us (68%)
  matrix products  26.6 us (10%)
  starting transfers between devices  18.1 us (7%)
  other arithmetic  16.8 us (6%)
  between operations  13.3 us (5%)
  local copies, waits for them, and re-layouts  10.7 us (4%)
    all_to_all x2, waiting for transfers between devices, sent_to_all(): lax.all_to_all(jnp.broadcast_to(value[None], (count, *value.shape)), axis...  76.5 us
    all_gather x2, waiting for transfers between devices, in_one_piece(): lax.all_gather(both, axis, axis=dim, tiled=True)  69.8 us
    reduce_scatter x1, waiting for transfers between devices, on_device(): lax.psum_scatter(lax.dot_general(product, down_full, (((1,), (1,)), ((),...  40.2 us
    dot_general x1, matrix products, on_device(): lax.dot_general(product, down_full, (((1,), (1,)), ((), ())), preferred_e...  13.3 us
    all_to_all x2, starting transfers between devices, sent_to_all(): lax.all_to_all(jnp.broadcast_to(value[None], (count, *value.shape)), axis...  8.95 us
    all_to_all x1, starting transfers between devices, on_device(): lax.all_to_all(jnp.stack([out_weight] * lax.axis_size('fs')), 'fs', 0, 0)  8.91 us
    dot_general x1, matrix products, on_device(): jnp.dot(normed_ffn, ffgate_full, preferred_element_type=jnp.float32)  6.39 us
    reduce_sum x2, other arithmetic, row_norm(): jnp.mean(floats * floats, axis=-1, keepdims=True) + norm_floor  6.2 us
  transfers between devices with their start and end apart: 6, of which 5 were waited for; matrix products, arithmetic and copies ran while one was open for 11% of the time, Pallas kernels for 0%

profile of v1, /device:TPU:2, one launch (start us, length us, event | category | flops | bytes accessed | tf_op | source)
XLA Modules:
  0.0 272.1 jit_solution(8109473629037071336)
XLA Ops:
  6.5 0.0 all-gather.3.cloned.1.call-start
  6.5 1.4 pad_maximum_fusion.1
  7.9 0.0 all-gather.3.cloned.1.call-update
  8.0 0.0 all-gather.5.cloned.1.call-start
  8.0 2.0 pad_maximum_fusion
  10.0 0.0 all-gather.5.cloned.1.call-update
  10.0 1.6 stack.2
  11.6 8.9 %all-to-all-start.1 = ((bf16[16,64,256]{2,1,0:T(8,128)(2,1)}), bf16[16,64,256]{2,1,0:T(8,128)(2,1)S(1)}, u32[]{:S(2)}, u32[]{:S(2)}) async-start(bf16[16,64,256]{2,1,0:T(8,128)(2,1)} %stack.2), calls=%async_computation.1 | async-start | bytes 1048576 | tf_op jit(solution)/shard_map/all_to_all | solution.py:79
  20.5 0.7 convert_element_type.73
  21.2 0.7 convert_element_type.70
  21.9 0.7 convert_element_type.72
  22.6 3.1 %fusion = f32[1024]{0:T(1024)S(1)} fusion(bf16[1,1024,2048]{2,1,0:T(8,128)(2,1)} %param.12), kind=kLoop, calls=%fused_computation.2 | loop fusion | flops 6290432 | bytes 4198400 | tf_op jit(solution)/shard_map/reduce_sum | solution.py:38
  25.7 67.0 %all-gather.3.cloned.1.call-done = bf16[2048,256]{1,0:T(8,128)(2,1)} async-done(((bf16[128,256]{1,0:T(8,128)(2,1)}), bf16[2048,256]{1,0:T(8,128)(2,1)}) %all-gather.3.cloned.1.call-update) | async-done | bytes 1048592 | tf_op jit(solution)/shard_map/all_gather | solution.py:12
  92.7 0.0 copy-start
  92.7 0.0 copy-start.3
  92.7 3.8 %fusion.19 = f32[1024,128]{1,0:T(8,128)S(1)} fusion(bf16[1,1024,2048]{2,1,0:T(8,128)(2,1)} %param.12, f32[2048]{0:T(1024)S(1)} %convert_element_type.70, f32[1024]{0:T(1024)S(1)} %add_rsqrt_fusion.2, bf16[2048,256]{1,0:T(8,128)(2,1)} %all-gather.3.cloned.1.call-done), kind=kOutput, calls=%fused_computation.24 | convolution fusion | flops 545652736 | bytes 5255168 | tf_op jit(solution)/shard_map/dot_general | solution.py:84
  96.5 0.0 copy-done
  96.5 0.1 copy-done.3
  96.6 1.3 convolution_multiply_fusion
  97.9 2.3 fusion.48
  100.2 0.4 multiply_reduce_fusion.1
  100.6 0.4 multiply_convert_fusion.5
  101.0 0.1 copy.14
  101.1 0.0 all-to-all-done.1
  101.2 1.6 broadcast_in_dim.6
  102.7 4.3 %all-to-all-start = ((bf16[8,1024,128]{1,2,0:T(8,128)(2,1)}), bf16[8,1024,128]{1,2,0:T(8,128)(2,1)S(1)}, u32[]{:S(2)}, u32[]{:S(2)}) async-start(bf16[8,1024,128]{1,2,0:T(8,128)(2,1)} %broadcast_in_dim.6), calls=%async_computation | async-start | bytes 4194304 | tf_op jit(solution)/shard_map/all_to_all | solution.py:27
  107.0 27.2 %all-to-all-done = bf16[8,1024,128]{1,2,0:T(8,128)(2,1)S(1)} async-done(((bf16[8,1024,128]{1,2,0:T(8,128)(2,1)}), bf16[8,1024,128]{1,2,0:T(8,128)(2,1)S(1)}, u32[]{:S(2)}, u32[]{:S(2)}) %all-to-all-start) | async-done | bytes 2097184 | tf_op jit(solution)/shard_map/all_to_all | solution.py:27
  134.2 1.8 fusion.16
  136.0 2.3 broadcast_in_dim.7
  138.3 0.0 copy-start.2
  138.3 0.0 copy-start.1
  138.3 4.7 %all-to-all-start.2 = ((bf16[8,1024,256]{2,1,0:T(8,128)(2,1)}), bf16[8,1024,256]{2,1,0:T(8,128)(2,1)}, u32[]{:S(2)}, u32[]{:S(2)}) async-start(bf16[8,1024,256]{2,1,0:T(8,128)(2,1)} %broadcast_in_dim.7), calls=%async_computation.2 | async-start | bytes 8388608 | tf_op jit(solution)/shard_map/all_to_all | solution.py:27
  143.0 0.2 reduce-scatter.2.cloned.1.call-start
  143.3 0.0 copy-done.2
  143.3 0.0 copy-done.1
  143.3 49.3 %all-to-all-done.2 = bf16[8,1024,256]{2,1,0:T(8,128)(2,1)} async-done(((bf16[8,1024,256]{2,1,0:T(8,128)(2,1)}), bf16[8,1024,256]{2,1,0:T(8,128)(2,1)}, u32[]{:S(2)}, u32[]{:S(2)}) %all-to-all-start.2) | async-done | bytes 4194336 | tf_op jit(solution)/shard_map/all_to_all | solution.py:27
  192.7 4.9 %copy.16 = bf16[8,128,8,256]{3,2,0,1:T(8,128)(2,1)} copy(bf16[8,128,8,256]{3,2,1,0:T(8,128)(2,1)} %bitcast.41) | data formatting | bytes 8388608 | tf_op jit(solution)/shard_map/reshape | solution.py:22
  197.5 3.1 %multiply_reduce_fusion = f32[1024]{0:T(1024)S(1)} fusion(bf16[8,1024,256]{2,1,0:T(8,128)(2,1)} %all-to-all-done.2), kind=kLoop, calls=%fused_computation.6 | loop fusion | flops 6290432 | bytes 4198400 | tf_op jit(solution)/shard_map/reduce_sum | solution.py:38
  200.7 2.8 %all-gather.5.cloned.1.call-done = bf16[2048,2304]{1,0:T(8,128)(2,1)} async-done(((bf16[128,2304]{1,0:T(8,128)(2,1)}), bf16[2048,2304]{1,0:T(8,128)(2,1)}) %all-gather.5.cloned.1.call-update) | async-done | bytes 9437200 | tf_op jit(solution)/shard_map/all_gather | solution.py:12
  203.5 6.4 %fusion.6 = f32[1024,768]{1,0:T(8,128)S(1)} fusion(bf16[2048,2304]{1,0:T(8,128)(2,1)} %all-gather.5.cloned.1.call-done, bf16[1024,2048]{1,0:T(8,128)(2,1)} %bitcast.83, f32[2048]{0:T(1024)S(1)} %convert_element_type.79, f32[1024]{0:T(1024)S(1)} %add_rsqrt_fusion), kind=kOutput, calls=%fused_computation.11 | convolution fusion | flops 3229614080 | bytes 10498048 | tf_op jit(solution)/shard_map/dot_general | solution.py:97
  209.9 13.3 %convolution_convert_fusion = bf16[1024,2048]{1,0:T(8,128)(2,1)} fusion(bf16[2048,2304]{1,0:T(8,128)(2,1)} %all-gather.5.cloned.1.call-done, f32[1024,768]{1,0:T(8,128)S(1)} %fusion.6, f32[768]{0:T(1024)S(1)} %get-tuple-element.6, f32[768]{0:T(1024)S(1)} %get-tuple-element.7, f32[768]{0:T(1024)S(1)} %get-tuple-element.5, bf16[1024,2048]{1,0:T(8,128)(2,1)} %bitcast.84, ...), kind=kOutput, calls=%fused_computation.7 | convolution fusion | flops 6461587456 | bytes 17847296 | tf_op jit(solution)/shard_map/dot_general | solution.py:104
  223.2 0.0 reduce-scatter.2.cloned.1.call-update
  223.2 40.2 %reduce-scatter.2.cloned.1.call-done = bf16[128,2048]{1,0:T(8,128)(2,1)} async-done(((bf16[1024,2048]{1,0:T(8,128)(2,1)}), bf16[128,2048]{1,0:T(8,128)(2,1)}) %reduce-scatter.2.cloned.1.call-update) | async-done | bytes 524304 | tf_op jit(solution)/shard_map/reduce_scatter | solution.py:103
  263.4 2.1 fusion.22
  (9 shorter events, 0.1 us)
Async XLA Ops:
  6.5 86.2 %all-gather.3.cloned.1.call-start = ((), (), s32[]{:S(2)}) async-start(), calls=%async_computation.4 | async-start | bytes 1114112 | tf_op jit(solution)/shard_map/all_gather | solution.py:12
  8.0 195.5 %all-gather.5.cloned.1.call-start = ((), (), s32[]{:S(2)}) async-start(), calls=%async_computation.5 | async-start | bytes 10027008 | tf_op jit(solution)/shard_map/all_gather | solution.py:12
  11.6 89.5 %all-to-all-start.1 = ((bf16[16,64,256]{2,1,0:T(8,128)(2,1)}), bf16[16,64,256]{2,1,0:T(8,128)(2,1)S(1)}, u32[]{:S(2)}, u32[]{:S(2)}) async-start(bf16[16,64,256]{2,1,0:T(8,128)(2,1)} %stack.2), calls=%async_computation.1 | async-start | bytes 1048576 | tf_op jit(solution)/shard_map/all_to_all | solution.py:79
  92.7 3.8 %copy-start = (bf16[1,1024,2048]{2,1,0:T(8,128)(2,1)S(1)}, bf16[1,1024,2048]{2,1,0:T(8,128)(2,1)}, u32[]{:S(2)}) copy-start(bf16[1,1024,2048]{2,1,0:T(8,128)(2,1)} %param.12) | copy-start | bytes 12582916
  92.7 3.9 %copy-start.3 = (bf16[2048,256]{1,0:T(8,128)(2,1)S(1)}, bf16[2048,256]{1,0:T(8,128)(2,1)}, u32[]{:S(2)}) copy-start(bf16[2048,256]{1,0:T(8,128)(2,1)} %all-gather.3.cloned.1.call-done) | copy-start | bytes 3145732
  102.7 31.4 %all-to-all-start = ((bf16[8,1024,128]{1,2,0:T(8,128)(2,1)}), bf16[8,1024,128]{1,2,0:T(8,128)(2,1)S(1)}, u32[]{:S(2)}, u32[]{:S(2)}) async-start(bf16[8,1024,128]{1,2,0:T(8,128)(2,1)} %broadcast_in_dim.6), calls=%async_computation | async-start | bytes 4194304 | tf_op jit(solution)/shard_map/all_to_all | solution.py:27
  138.3 4.9 %copy-start.2 = (bf16[2048]{0:T(1024)(128)(2,1)S(1)}, bf16[2048]{0:T(1024)(128)(2,1)}, u32[]{:S(2)}) copy-start(bf16[2048]{0:T(1024)(128)(2,1)} %param.19) | copy-start | bytes 12292
  138.3 4.9 %copy-start.1 = (bf16[3,768]{1,0:T(4,128)(2,1)S(1)}, bf16[3,768]{1,0:T(4,128)(2,1)}, u32[]{:S(2)}) copy-start(bf16[3,768]{1,0:T(4,128)(2,1)} %param.22) | copy-start | bytes 13828
  138.3 54.3 %all-to-all-start.2 = ((bf16[8,1024,256]{2,1,0:T(8,128)(2,1)}), bf16[8,1024,256]{2,1,0:T(8,128)(2,1)}, u32[]{:S(2)}, u32[]{:S(2)}) async-start(bf16[8,1024,256]{2,1,0:T(8,128)(2,1)} %broadcast_in_dim.7), calls=%async_computation.2 | async-start | bytes 8388608 | tf_op jit(solution)/shard_map/all_to_all | solution.py:27
  143.0 120.4 %reduce-scatter.2.cloned.1.call-start = ((), (), s32[]{:S(2)}) async-start(), calls=%async_computation.6 | async-start | bytes 4718592 | tf_op jit(solution)/shard_map/reduce_scatter | solution.py:103
Sparse Core Ops, SparseCore 0:
  9.1 83.5 all-gather.2
  94.5 108.9 all-gather.4
  223.4 40.0 reduce-scatter.1
